TPU v7x, 32 devices: a whole 2x2x4 slice. The times are simulated.
32 devices in a mesh: grp: 2 (over x), ep: 4 (over y, core), tp: 4 (over z).
Axes of the slice: x: 2, y: 2, z: 4, core: 2. Of those that a mesh axis runs over, the one named last changes fastest.
Arguments:
- tokens: bfloat16 [2048, 4096], P(('grp', 'ep')), parts along dimension 0, may hold values from -6 to 6
- expert_ids: int32 [2048, 2], P(('grp', 'ep')), parts along dimension 0, may hold values from 0 to 15, as said below
- gates: float32 [2048, 2], P(('grp', 'ep')), parts along dimension 0, may hold values from 0.1 to 1
- w_gate: bfloat16 [16, 4096, 2048], P('ep', None, 'tp'), may hold values from -0.09375 to 0.09375
- w_up: bfloat16 [16, 4096, 2048], P('ep', None, 'tp'), may hold values from -0.09375 to 0.09375
- w_down: bfloat16 [16, 2048, 4096], P('ep', 'tp'), may hold values from -0.79549513 to 0.79549513, as said below
- norm_gain: float32 [4096], P('tp'), may hold values from 0.1 to 1.9
- norm_bias: float32 [4096], P('tp'), may hold values from -1.5 to 1.5
Outputs:
- normed: bfloat16 [2048, 4096], P(('grp', 'ep'), 'tp'), parts along dimension 0
There are 2 independent parts, one for each index of `grp`. A program takes and returns all parts, laid end to end along the dimension named above; an argument that names none is the same for every part. Nothing has to cross between parts.
Inputs may be any that keep to these rules, and one draw needn't show every extreme that they name: `expert_ids`: each row names 2 different experts, both in the same group of 4 consecutive expert numbers. Within one aligned block of 256 rows no expert is named more than 64 times, and in every draw some expert is named exactly 64 times in every block. `w_down`: down projection weights.
All inputs are finite; a program needn't handle non-finite values.
Results may differ from a plain program's by a relative error of at most 0.014.
Values may be sent and summed in bfloat16 or wider, within the bound.
A program may use at most 128 MiB of HBM per device.

v0:
```python
import jax
import jax.numpy as jnp
from jax import lax
from jax.sharding import PartitionSpec as P

D = 4096
TOPK = 2
EXPERTS = 16
CAP = 64


norm_eps = 1e-05


def route_slots(expert_ids):
    flat_ids = expert_ids.reshape(-1)
    onehot = (flat_ids[:, None] == jnp.arange(EXPERTS, dtype=jnp.int32)[None, :]).astype(jnp.int32)
    position = jnp.sum((jnp.cumsum(onehot, axis=0) - 1) * onehot, axis=1)
    target = flat_ids * CAP + position
    token_of = jnp.arange(flat_ids.shape[0], dtype=jnp.int32) // TOPK
    source = jnp.zeros((EXPERTS * CAP,), jnp.int32).at[target].set(token_of)
    filled = jnp.zeros((EXPERTS * CAP,), jnp.bool_).at[target].set(True)
    return (target, source, filled)


def on_device(tokens, expert_ids, gates, w_gate, w_up, w_down, norm_gain, norm_bias):
    tok_rows, width = tokens.shape
    piece_width = norm_gain.shape[0]
    target, source, filled = route_slots(expert_ids)
    outgoing = jnp.where(filled[:, None], tokens[source], jnp.zeros((), jnp.bfloat16)).reshape(
        EXPERTS, CAP, width
    )
    arrived = lax.all_to_all(outgoing, "ep", split_axis=0, concat_axis=1, tiled=True)
    gate_part = jnp.einsum("erd,edf->erf", arrived, w_gate, preferred_element_type=jnp.float32)
    up_part = jnp.einsum("erd,edf->erf", arrived, w_up, preferred_element_type=jnp.float32)
    hidden = (jax.nn.silu(gate_part) * up_part).astype(jnp.bfloat16)
    partial_value = jnp.einsum("erf,efd->erd", hidden, w_down, preferred_element_type=jnp.float32)
    summed = lax.psum_scatter(
        partial_value.astype(jnp.bfloat16), "tp", scatter_dimension=2, tiled=True
    )
    returned = lax.all_to_all(summed, "ep", split_axis=1, concat_axis=0, tiled=True)
    picked = returned.reshape(EXPERTS * CAP, piece_width)[target].reshape(
        tok_rows, TOPK, piece_width
    )
    combined = jnp.sum(picked.astype(jnp.float32) * gates[:, :, None], axis=1)
    stats = lax.psum((jnp.sum(combined, axis=1), jnp.sum(combined * combined, axis=1)), "tp")
    row_mean = stats[0] / D
    row_var = stats[1] / D - row_mean * row_mean
    normed = (combined - row_mean[:, None]) * lax.rsqrt(
        row_var[:, None] + norm_eps
    ) * norm_gain + norm_bias
    return normed.astype(jnp.bfloat16)


def solution(mesh):
    return jax.shard_map(
        on_device,
        mesh=mesh,
        in_specs=(
            P(("grp", "ep"), None),
            P(("grp", "ep"), None),
            P(("grp", "ep"), None),
            P("ep", None, "tp"),
            P("ep", None, "tp"),
            P("ep", "tp", None),
            P("tp"),
            P("tp"),
        ),
        out_specs=P(("grp", "ep"), "tp"),
        check_vma=False,
    )
```

profile of v0, /device:TPU:0, one launch (start us, length us, event | category | flops | bytes accessed | tf_op | source)
XLA Modules:
  0.0 389.8 jit_solution(9872680368133698171)
XLA Ops:
  6.5 1.0 copy.20
  7.8 0.7 broadcast_multiply_fusion
  8.5 1.2 reduce-window.6
  9.6 0.2 slice_reduce_fusion
  10.3 2.4 scatter_custom_fusion.1
  12.8 2.4 scatter_custom_fusion
  15.3 7.8 %gather_fusion = bf16[1024,4096]{1,0:T(8,128)(2,1)} fusion(bf16[256,4096]{1,0:T(8,128)(2,1)S(1)} %copy-done, s32[1024]{0:T(1024)S(1)} %fusion.4), kind=kCustom, calls=%fused_computation | custom fusion | bytes 16781312 | tf_op jit(solution)/shard_map/gather | solution.py:30
  23.1 7.2 %broadcast_select_fusion = bf16[16,64,4096]{2,1,0:T(8,128)(2,1)} fusion(bf16[16,64,4096]{2,1,0:T(8,128)(2,1)} %bitcast.32, pred[16,64]{1,0:T(8,128)(4,1)S(1)} %broadcast_in_dim.35), kind=kLoop, calls=%fused_computation.4 | loop fusion | flops 4194304 | bytes 16778240 | tf_op jit(solution)/shard_map/jit(_where)/select_n | solution.py:30
  30.4 101.4 %all_to_all.33 = bf16[16,64,4096]{2,1,0:T(8,128)(2,1)} all-to-all(bf16[16,64,4096]{2,1,0:T(8,128)(2,1)} %broadcast_select_fusion), channel_id=1, replica_groups=mesh['grp'=2,'ep'=4,'tp'=4] {'ep'}, dimensions={0} | all-to-all | bytes 16777216 | tf_op jit(solution)/shard_map/all_to_all | solution.py:33
  131.8 7.7 %copy.23 = bf16[4,4,64,4096]{3,2,1,0:T(8,128)(2,1)} copy(bf16[4,4,64,4096]{3,2,0,1:T(8,128)(2,1)} %bitcast.35) | data formatting | bytes 16777216 | tf_op jit(solution)/shard_map/all_to_all | solution.py:33
  139.5 10.5 %fusion.13 = f32[4,256,512]{2,1,0:T(8,128)S(1)} fusion(bf16[4,256,4096]{2,1,0:T(8,128)(2,1)} %bitcast.33, bf16[4,4096,512]{2,1,0:T(8,128)(2,1)} %param.11), kind=kOutput, calls=%fused_computation.39 | convolution fusion | flops 4294967296 | bytes 27262976 | tf_op jit(solution)/shard_map/erd,edf->erf/dot_general | solution.py:34
  150.0 24.9 %convolution_convert_fusion = bf16[4,256,4096]{2,1,0:T(8,128)(2,1)} fusion(bf16[4,512,4096]{2,1,0:T(8,128)(2,1)} %param.13, f32[4,256,512]{2,1,0:T(8,128)S(1)} %fusion.13, bf16[4,256,4096]{2,1,0:T(8,128)(2,1)} %bitcast.34, bf16[4,4096,512]{2,1,0:T(8,128)(2,1)} %param.12), kind=kOutput, calls=%fused_computation.5 | convolution fusion | flops 8597274624 | bytes 52428800 | tf_op jit(solution)/shard_map/erf,efd->erd/dot_general | solution.py:37
  175.0 145.7 %reduce-scatter.2.cloned.1.call-done = bf16[4,256,1024]{2,1,0:T(8,128)(2,1)} async-done(((bf16[4,256,4096]{2,1,0:T(8,128)(2,1)}), bf16[4,256,1024]{2,1,0:T(8,128)(2,1)}) %reduce-scatter.2.cloned.1.call-update) | async-done | bytes 2097168 | tf_op jit(solution)/shard_map/reduce_scatter | solution.py:38
  320.7 4.5 %copy.24 = bf16[4,256,1024]{2,0,1:T(4,128)(2,1)} copy(bf16[4,256,1024]{2,1,0:T(8,128)(2,1)} %reduce-scatter.2.cloned.1.call-done) | data formatting | bytes 4194304 | tf_op jit(solution)/shard_map/reduce_scatter | solution.py:38
  325.2 3.8 all-to-all-start.1
  329.4 25.1 %all-to-all-done.1 = bf16[4,256,1024]{2,0,1:T(4,128)(2,1)S(1)} async-done(((bf16[4,256,1024]{2,0,1:T(4,128)(2,1)}), bf16[4,256,1024]{2,0,1:T(4,128)(2,1)S(1)}, u32[]{:S(2)}, u32[]{:S(2)}) %all-to-all-start.1) | async-done | bytes 2097184 | tf_op jit(solution)/shard_map/all_to_all | solution.py:41
  354.5 2.0 copy.25
  356.5 4.7 %gather_fusion.1 = bf16[512,1024]{1,0:T(8,128)(2,1)S(1)} fusion(bf16[1024,1024]{1,0:T(8,128)(2,1)} %bitcast.31, s32[1024]{0:T(1024)S(1)} %pad_clamp_fusion), kind=kCustom, calls=%fused_computation.1 | custom fusion | bytes 2099200 | tf_op jit(solution)/shard_map/gather | solution.py:42
  361.2 2.4 reshape.74
  363.6 4.3 %multiply_reduce_fusion.1 = f32[256,1024]{1,0:T(8,128)S(1)} fusion(f32[256,2,1024]{2,1,0:T(2,128)} %reshape.74, f32[256,2]{1,0:T(8,128)S(1)} %copy.26), kind=kLoop, calls=%fused_computation.7 | loop fusion | flops 786432 | bytes 3147776 | tf_op jit(solution)/shard_map/reduce_sum | solution.py:45
  367.9 1.0 copy-done.2
  369.0 0.3 multiply_reduce_fusion
  369.6 11.1 %all-reduce = (f32[256]{0:T(256)S(1)}, f32[256]{0:T(256)S(1)}) all-reduce(f32[256]{0:T(256)S(1)} %multiply_reduce_fusion.2, f32[256]{0:T(256)S(1)} %reduce_sum.50), channel_id=1, replica_groups=mesh['grp'=2,'ep'=4,'tp'=4] {'tp'}, use_global_device_ids=true, to_apply=%region_11.12 | all-reduce | flops 512 | bytes 4096 | tf_op jit(solution)/shard_map/psum | solution.py:46
  380.7 2.3 add_convert_fusion
  (33 shorter events, 1.5 us)
Async XLA Ops:
  6.5 8.8 %copy-start = (bf16[256,4096]{1,0:T(8,128)(2,1)S(1)}, bf16[256,4096]{1,0:T(8,128)(2,1)}, u32[]{:S(2)}) copy-start(bf16[256,4096]{1,0:T(8,128)(2,1)} %param.8) | copy-start | bytes 6291460
  6.5 314.2 %reduce-scatter.2.cloned.1.call-start = ((), (), s32[]{:S(2)}) async-start(), calls=%async_computation.3 | async-start | bytes 10485760 | tf_op jit(solution)/shard_map/reduce_scatter | solution.py:38
  174.9 154.1 %copy-start.5 = (f32[256,2]{0,1:T(2,128)S(1)}, f32[256,2]{0,1:T(2,128)}, u32[]{:S(2)}) copy-start(f32[256,2]{0,1:T(2,128)} %param.10) | copy-start | bytes 6148
  325.2 29.2 %all-to-all-start.1 = ((bf16[4,256,1024]{2,0,1:T(4,128)(2,1)}), bf16[4,256,1024]{2,0,1:T(4,128)(2,1)S(1)}, u32[]{:S(2)}, u32[]{:S(2)}) async-start(bf16[4,256,1024]{2,0,1:T(4,128)(2,1)} %copy.24), calls=%async_computation.2 | async-start | bytes 4194304 | tf_op jit(solution)/shard_map/all_to_all | solution.py:41
  356.5 26.5 %copy-start.1 = (bf16[256,4096]{1,0:T(8,128)(2,1)S(1)}, bf16[256,4096]{1,0:T(8,128)(2,1)}, u32[]{:S(2)}) copy-start(bf16[256,4096]{1,0:T(8,128)(2,1)} %param.8) | copy-start | bytes 6291460
  356.5 24.2 %copy-start.3 = (f32[1024]{0:T(1024)S(1)}, f32[1024]{0:T(1024)}, u32[]{:S(2)}) copy-start(f32[1024]{0:T(1024)} %param.15) | copy-start | bytes 12292
  356.5 24.2 %copy-start.4 = (f32[1024]{0:T(1024)S(1)}, f32[1024]{0:T(1024)}, u32[]{:S(2)}) copy-start(f32[1024]{0:T(1024)} %param.14) | copy-start | bytes 12292
  367.9 1.0 copy-start.2
Sparse Core Ops, SparseCore 0:
  175.1 145.5 reduce-scatter.1
where the time goes:
time: 390 us
  waiting for transfers between devices  171 us (44%)
  blocking collectives  112 us (29%)
  local copies, waits for them, and re-layouts  37.3 us (10%)
  matrix products  35.4 us (9%)
  other arithmetic  16.4 us (4%)
  between operations  13.5 us (3%)
    reduce_scatter x1, waiting for transfers between devices, on_device(): lax.psum_scatter(partial_value.astype(jnp.bfloat16), 'tp', scatter_dimens...  146 us
    all_to_all x1, blocking collectives, on_device(): lax.all_to_all(outgoing, 'ep', split_axis=0, concat_axis=1, tiled=True)  101 us
    all_to_all x1, waiting for transfers between devices, on_device(): lax.all_to_all(summed, 'ep', split_axis=1, concat_axis=0, tiled=True)  25.1 us
    dot_general x1, matrix products, on_device(): jnp.einsum('erf,efd->erd', hidden, w_down, preferred_element_type=jnp.flo...  24.9 us
    psum x1, blocking collectives, on_device(): lax.psum((jnp.sum(combined, axis=1), jnp.sum(combined * combined, axis=1)...  11.1 us
    dot_general x1, matrix products, on_device(): jnp.einsum('erd,edf->erf', arrived, w_gate, preferred_element_type=jnp.fl...  10.5 us
    gather x1, local copies, waits for them, and re-layouts, on_device(): tokens[source]  7.82 us
  transfers between devices with their start and end apart: 2, of which 2 were waited for; matrix products, arithmetic and copies ran while one was open for 0% of the time, Pallas kernels for 0%

commit v1 on v0

--- a/solution.py
+++ b/solution.py
@@ -1,6 +1,9 @@
+import functools
 import jax
 import jax.numpy as jnp
 from jax import lax
+from jax.experimental import pallas as pl
+from jax.experimental.pallas import tpu as pltpu
 from jax.sharding import PartitionSpec as P
 
 D = 4096
@@ -52,9 +55,366 @@
     return normed.astype(jnp.bfloat16)
 
 
+GROUP_EXPERTS = 4
+CHUNKS = 8
+HALF = CHUNKS // 2
+Z_OFFSETS = (2, 1, 3, 0)
+F32 = jnp.float32
+BF16 = jnp.bfloat16
+MESH = pl.DeviceIdType.MESH
+
+
+def moe_kernel(
+    ids_ref, gates_ref, gain_ref, bias_ref, tokens_ref, wg_ref, wu_ref, wd_ref,
+    out_ref,
+    tok, wbuf, wd, acc, hid, xr, dnb, place, collect, rowg, meta, meta_in,
+    part, core_in, y_in, z_in, st_out, st_in,
+    tok_sem, y_send, y_recv, z_send, z_recv, own_send, own_recv, fwd_send, fwd_recv,
+    meta_send, meta_recv, w_sem, wd_sem, pc_send, pc_recv, py_send, py_recv,
+    pz_send, pz_recv, st_send, st_recv,
+):
+    ep = lax.axis_index("ep")
+    z = lax.axis_index("tp")
+    y, c = ep // 2, ep % 2
+    partner = y * 2 + (1 - c)
+    across = (1 - y) * 2 + c
+    diag = (1 - y) * 2 + (1 - c)
+    par = z % 2
+    zpeer = z + 1 - 2 * par
+    rows, width = tokens_ref.shape
+    experts = wg_ref.shape[0]
+    cols = width // CHUNKS
+    piece = gain_ref.shape[1]
+
+    def remote(src, dst, send, recv, e, t):
+        return pltpu.make_async_remote_copy(
+            src_ref=src, dst_ref=dst, send_sem=send, recv_sem=recv,
+            device_id={"ep": e, "tp": t}, device_id_type=MESH,
+        )
+
+    def span(ch, size):
+        return pl.ds(pl.multiple_of(ch * size, size), size)
+
+    def load_tok(ch):
+        return pltpu.make_async_copy(
+            tokens_ref.at[:, span(ch, cols)], tok.at[ch, ep], tok_sem.at[ch])
+
+    def load_w(ch, slot):
+        return (
+            pltpu.make_async_copy(
+                wg_ref.at[:, span(ch, cols), :], wbuf.at[slot, 0], w_sem.at[slot, 0]),
+            pltpu.make_async_copy(
+                wu_ref.at[:, span(ch, cols), :], wbuf.at[slot, 1], w_sem.at[slot, 1]),
+        )
+
+    def load_wd(i):
+        q = (z + Z_OFFSETS[i]) % 4
+        return pltpu.make_async_copy(
+            wd_ref.at[:, :, span(q, piece)], wd.at[i], wd_sem.at[i])
+
+    def direct(j):
+        return par * HALF + j
+
+    def swapped(j):
+        return (1 - par) * HALF + j
+
+    def y_copy(j):
+        blk = tok.at[direct(j), ep]
+        return remote(blk, blk, y_send.at[j], y_recv.at[j], across, z)
+
+    def y_arrive(j):
+        blk = tok.at[direct(j), across]
+        return remote(blk, blk, y_send.at[j], y_recv.at[j], across, z)
+
+    def z_copy(j):
+        blk = tok.at[direct(j), across]
+        return remote(blk, blk, z_send.at[j], z_recv.at[j], ep, zpeer)
+
+    def z_arrive(j):
+        blk = tok.at[swapped(j), across]
+        return remote(blk, blk, z_send.at[j], z_recv.at[j], ep, zpeer)
+
+    def own_copy(ch):
+        blk = tok.at[ch, ep]
+        return remote(blk, blk, own_send.at[ch], own_recv.at[ch], partner, z)
+
+    def own_arrive(ch):
+        blk = tok.at[ch, partner]
+        return remote(blk, blk, own_send.at[ch], own_recv.at[ch], partner, z)
+
+    def fwd_copy(ch):
+        blk = tok.at[ch, across]
+        return remote(blk, blk, fwd_send.at[ch], fwd_recv.at[ch], partner, z)
+
+    def fwd_arrive(ch):
+        blk = tok.at[ch, diag]
+        return remote(blk, blk, fwd_send.at[ch], fwd_recv.at[ch], partner, z)
+
+    def meta_copy(e, k):
+        return remote(meta.at[e], meta_in.at[ep], meta_send.at[k], meta_recv.at[k], e, z)
+
+    def meta_arrive(e, k):
+        return remote(meta.at[e], meta_in.at[e], meta_send.at[k], meta_recv.at[k], e, z)
+
+    peers = (partner, across, diag)
+
+    for j in range(HALF):
+        load_tok(direct(j)).start()
+    for j in range(HALF):
+        load_tok(swapped(j)).start()
+
+    barrier = pltpu.get_barrier_semaphore()
+    for e in peers:
+        pl.semaphore_signal(barrier, inc=1, device_id={"ep": e, "tp": z}, device_id_type=MESH)
+    for d in (1, 2, 3):
+        pl.semaphore_signal(
+            barrier, inc=1, device_id={"ep": ep, "tp": (z + d) % 4}, device_id_type=MESH)
+    pl.semaphore_wait(barrier, 6)
+
+    for j in range(HALF):
+        load_tok(direct(j)).wait()
+        y_copy(j).start()
+        own_copy(direct(j)).start()
+    for j in range(HALF):
+        load_tok(swapped(j)).wait()
+        own_copy(swapped(j)).start()
+    for cp in load_w(direct(0), 0) + load_w(swapped(0), 1):
+        cp.start()
+    for i in range(4):
+        load_wd(i).start()
+
+    lane = lax.broadcasted_iota(jnp.int32, (rows, 128), 1)
+    first = ids_ref[:, 0:1] == lane
+    second = ids_ref[:, 1:2] == lane
+    named = jnp.where(first | second, 1.0, 0.0).astype(F32)
+    weight = jnp.where(first, gates_ref[:, 0:1], jnp.where(second, gates_ref[:, 1:2], 0.0))
+    tri_r = lax.broadcasted_iota(jnp.int32, (rows, rows), 0)
+    tri_c = lax.broadcasted_iota(jnp.int32, (rows, rows), 1)
+    before = jnp.where(tri_c < tri_r, 1.0, 0.0).astype(BF16)
+    position = jnp.dot(before, named.astype(BF16), preferred_element_type=F32)
+    slot = jnp.where(named > 0.5, position + ((lane % experts) * CAP).astype(F32), -1.0)
+    slot_t = slot.T
+    weight_t = weight.T
+    for e in range(4):
+        meta[e, 0:experts, :] = slot_t[e * experts:(e + 1) * experts, :]
+        meta[e, experts:2 * experts, :] = weight_t[e * experts:(e + 1) * experts, :]
+    for k, e in enumerate(peers):
+        meta_copy(e, k).start()
+    meta_in[ep] = meta[ep]
+    acc[...] = jnp.zeros_like(acc)
+    for k, e in enumerate(peers):
+        meta_arrive(e, k).wait_recv()
+
+    row_f = tri_r.astype(F32)
+    for s in range(4):
+        info = meta_in[s]
+        put = jnp.zeros((rows, rows), F32)
+        for e in range(experts):
+            put += jnp.where(row_f == info[e:e + 1, :], 1.0, 0.0)
+        place[s] = put.astype(BF16)
+        collect[s] = put.T.astype(BF16)
+        for e in range(experts):
+            g = jnp.sum(
+                put[e * CAP:(e + 1) * CAP, :] * info[experts + e:experts + e + 1, :],
+                axis=1, keepdims=True)
+            rowg[e, s * CAP:(s + 1) * CAP, :] = jnp.broadcast_to(g, (CAP, 128))
+
+    def work(ch, slot_no):
+        for s in range(4):
+            x = jnp.dot(place[s], tok[ch, s], preferred_element_type=F32).astype(BF16)
+            for e in range(experts):
+                xr[e, s * CAP:(s + 1) * CAP, :] = x[e * CAP:(e + 1) * CAP, :]
+        for cp in load_w(ch, slot_no):
+            cp.wait()
+
+        def one(e, carry):
+            for k in range(2):
+                acc[k, e] += jnp.dot(xr[e], wbuf[slot_no, k, e], preferred_element_type=F32)
+            return carry
+        lax.fori_loop(0, experts, one, 0)
+
+    def step(j, carry):
+        @pl.when(j < HALF)
+        def _():
+            y_arrive(j).wait_recv()
+            z_copy(j).start()
+            fwd_copy(direct(j)).start()
+
+        @pl.when(j >= 1)
+        def _():
+            z_arrive(j - 1).wait_recv()
+            fwd_copy(swapped(j - 1)).start()
+
+        @pl.when(j < HALF)
+        def _():
+            ch = direct(j)
+            own_arrive(ch).wait_recv()
+            fwd_arrive(ch).wait_recv()
+            work(ch, 0)
+
+            @pl.when(j < HALF - 1)
+            def _():
+                for cp in load_w(direct(j + 1), 0):
+                    cp.start()
+
+        @pl.when(j >= 1)
+        def _():
+            ch = swapped(j - 1)
+            own_arrive(ch).wait_recv()
+            fwd_arrive(ch).wait_recv()
+            work(ch, 1)
+
+            @pl.when(j < HALF)
+            def _():
+                for cp in load_w(swapped(j), 1):
+                    cp.start()
+        return carry
+    lax.fori_loop(0, HALF + 1, step, 0)
+
+    def activate(e, carry):
+        g = acc[0, e]
+        h = g / (1.0 + jnp.exp(-g)) * acc[1, e]
+        hid[e] = (h * rowg[e][:, 0:1]).astype(BF16)
+        return carry
+    lax.fori_loop(0, experts, activate, 0)
+
+    def core_copy(i):
+        return remote(part.at[i, 1 - c], core_in.at[i], pc_send.at[i], pc_recv.at[i], partner, z)
+
+    def ret_copy(i):
+        return remote(part.at[i, c, 1 - y], y_in.at[i], py_send.at[i], py_recv.at[i], across, z)
+
+    def scatter_copy(i):
+        q = (z + Z_OFFSETS[i]) % 4
+        return remote(part.at[i, c, y], z_in.at[i], pz_send.at[i], pz_recv.at[i], ep, q)
+
+    for i in range(5):
+        if i < 4:
+            load_wd(i).wait()
+
+            def down(e, carry):
+                o = jnp.dot(hid[e], wd[i, e], preferred_element_type=F32).astype(BF16)
+                for s in range(4):
+                    dnb[s, span(e, CAP), :] = o[s * CAP:(s + 1) * CAP, :]
+                return carry
+            lax.fori_loop(0, experts, down, 0)
+
+            def gather(s, carry):
+                part[i, s % 2, s // 2] = jnp.dot(
+                    collect[s], dnb[s], preferred_element_type=F32).astype(BF16)
+                return carry
+            lax.fori_loop(0, 4, gather, 0)
+            core_copy(i).start()
+        if i >= 1:
+            core_copy(i - 1).wait_recv()
+            part[i - 1, c, 1 - y] += core_in[i - 1, 1 - y]
+            ret_copy(i - 1).start()
+
+    for i in range(3):
+        ret_copy(i).wait_recv()
+        part[i, c, y] += core_in[i, y] + y_in[i]
+        scatter_copy(i).start()
+    ret_copy(3).wait_recv()
+    total = (part[3, c, y] + core_in[3, y] + y_in[3]).astype(F32)
+    for i in range(3):
+        scatter_copy(i).wait_recv()
+        total += z_in[i].astype(F32)
+
+    local_mean = jnp.sum(total, axis=1, keepdims=True) * (1.0 / piece)
+    gap = total - local_mean
+    local_m2 = jnp.sum(gap * gap, axis=1, keepdims=True)
+    mean_t = jnp.broadcast_to(local_mean, (rows, 128)).T
+    m2_t = jnp.broadcast_to(local_m2, (rows, 128)).T
+    st_out[0:8, :] = mean_t[0:8, :]
+    st_out[8:16, :] = m2_t[0:8, :]
+
+    def stat_copy(d):
+        return remote(
+            st_out, st_in.at[d - 1], st_send.at[d - 1], st_recv.at[d - 1], ep, (z + d) % 4)
+    for d in (1, 2, 3):
+        stat_copy(d).start()
+    for d in (1, 2, 3):
+        stat_copy(d).wait_recv()
+    means = [st_out[0:8, :]] + [st_in[d, 0:8, :] for d in range(3)]
+    m2s = [st_out[8:16, :]] + [st_in[d, 8:16, :] for d in range(3)]
+    mean = (means[0] + means[1] + means[2] + means[3]) * 0.25
+    m2 = m2s[0] + m2s[1] + m2s[2] + m2s[3]
+    for m in means:
+        m2 += (m - mean) * (m - mean) * piece
+    scale = lax.rsqrt(m2 * (1.0 / width) + norm_eps)
+    mean_col = jnp.broadcast_to(mean[0:1, :], (128, rows)).T[:, 0:1]
+    scale_col = jnp.broadcast_to(scale[0:1, :], (128, rows)).T[:, 0:1]
+    out_ref[...] = (
+        (total - mean_col) * scale_col * gain_ref[...] + bias_ref[...]).astype(BF16)
+
+    for j in range(HALF):
+        y_copy(j).wait_send()
+        z_copy(j).wait_send()
+    for ch in range(CHUNKS):
+        own_copy(ch).wait_send()
+        fwd_copy(ch).wait_send()
+    for k, e in enumerate(peers):
+        meta_copy(e, k).wait_send()
+    for i in range(4):
+        core_copy(i).wait_send()
+        ret_copy(i).wait_send()
+    for i in range(3):
+        scatter_copy(i).wait_send()
+    for d in (1, 2, 3):
+        stat_copy(d).wait_send()
+
+
+def fused_on_device(tokens, expert_ids, gates, w_gate, w_up, w_down, norm_gain, norm_bias):
+    rows, width = tokens.shape
+    experts, _, hidden = w_gate.shape
+    piece = norm_gain.shape[0]
+    cols = width // CHUNKS
+    dma = pltpu.SemaphoreType.DMA
+    vmem = pl.BlockSpec(memory_space=pltpu.VMEM)
+    hbm = pl.BlockSpec(memory_space=pl.ANY)
+    return pl.pallas_call(
+        moe_kernel,
+        out_shape=jax.ShapeDtypeStruct((rows, piece), jnp.bfloat16),
+        in_specs=[vmem] * 4 + [hbm] * 4,
+        out_specs=vmem,
+        scratch_shapes=[
+            pltpu.VMEM((CHUNKS, 4, rows, cols), BF16),
+            pltpu.VMEM((2, 2, experts, cols, hidden), BF16),
+            pltpu.VMEM((4, experts, hidden, piece), BF16),
+            pltpu.VMEM((2, experts, 4 * CAP, hidden), F32),
+            pltpu.VMEM((experts, 4 * CAP, hidden), BF16),
+            pltpu.VMEM((experts, 4 * CAP, cols), BF16),
+            pltpu.VMEM((4, experts * CAP, piece), BF16),
+            pltpu.VMEM((4, experts * CAP, rows), BF16),
+            pltpu.VMEM((4, rows, experts * CAP), BF16),
+            pltpu.VMEM((experts, 4 * CAP, 128), F32),
+            pltpu.VMEM((4, 2 * experts, rows), F32),
+            pltpu.VMEM((4, 2 * experts, rows), F32),
+            pltpu.VMEM((4, 2, 2, rows, piece), BF16),
+            pltpu.VMEM((4, 2, rows, piece), BF16),
+            pltpu.VMEM((4, rows, piece), BF16),
+            pltpu.VMEM((3, rows, piece), BF16),
+            pltpu.VMEM((16, rows), F32),
+            pltpu.VMEM((3, 16, rows), F32),
+            dma((CHUNKS,)), dma((HALF,)), dma((HALF,)), dma((HALF,)), dma((HALF,)),
+            dma((CHUNKS,)), dma((CHUNKS,)), dma((CHUNKS,)), dma((CHUNKS,)),
+            dma((3,)), dma((3,)), dma((2, 2)), dma((4,)),
+            dma((4,)), dma((4,)), dma((4,)), dma((4,)),
+            dma((3,)), dma((3,)), dma((3,)), dma((3,)),
+        ],
+        compiler_params=pltpu.CompilerParams(
+            collective_id=0, has_side_effects=True, vmem_limit_bytes=64 * 1024 * 1024 - 65536),
+    )(
+        expert_ids, gates, norm_gain[None, :], norm_bias[None, :],
+        tokens, w_gate, w_up, w_down,
+    )
+
+
 def solution(mesh):
+    groups_apart = EXPERTS == GROUP_EXPERTS * mesh.shape["ep"]
+    fused = groups_apart and mesh.shape["ep"] == 4 and mesh.shape["tp"] == 4
     return jax.shard_map(
-        on_device,
+        fused_on_device if fused else on_device,
         mesh=mesh,
         in_specs=(
             P(("grp", "ep"), None),

time: 390 us -> 137 us (0.35)
  waiting for transfers between devices: 171 us -> 0 us
  Pallas kernels: 0 us -> 132 us
  blocking collectives: 112 us -> 0 us
  matrix products: 35.4 us -> 0 us
  local copies, waits for them, and re-layouts: 37.3 us -> 4.81 us
  other arithmetic: 16.4 us -> 0 us
  between operations: 13.5 us -> 0.01 us
    reduce_scatter x1 -> x0, waiting for transfers between devices: 146 us -> none  [on_device(): lax.psum_scatter(partial_value.astype(jnp.bfloat16), 'tp', scatter_dimens...]
    pallas_call x0 -> x1, Pallas kernels: none -> 132 us  [fused_on_device(): pl.pallas_call(moe_kernel, out_shape=jax.ShapeDtypeStruct((rows, piece),...]
    all_to_all x1 -> x0, blocking collectives: 101 us -> none  [on_device(): lax.all_to_all(outgoing, 'ep', split_axis=0, concat_axis=1, tiled=True)]
    dot_general x2 -> x0, matrix products: 35.4 us -> none  [the longest x1 24.9 us: on_device(): jnp.einsum('erf,efd->erd', hidden, w_down, preferred_element_type=jnp.flo...]
    all_to_all x1 -> x0, waiting for transfers between devices: 25.1 us -> none  [on_device(): lax.all_to_all(summed, 'ep', split_axis=1, concat_axis=0, tiled=True)]
    gather x2 -> x0, local copies, waits for them, and re-layouts: 12.6 us -> none  [the longest x1 7.82 us: on_device(): tokens[source]]
    psum x1 -> x0, blocking collectives: 11.1 us -> none  [on_device(): lax.psum((jnp.sum(combined, axis=1), jnp.sum(combined * combined, axis=1)...]
    all_to_all x2 -> x0, local copies, waits for them, and re-layouts: 9.71 us -> none  [the longest x1 7.71 us: on_device(): lax.all_to_all(outgoing, 'ep', split_axis=0, concat_axis=1, tiled=True)]
  transfers between devices with their start and end apart: 2 -> 0, of which waited for: 2 -> 0; matrix products, arithmetic and copies ran while one was open for 0% -> 0% of each run, Pallas kernels for 0% -> 0%
where the time goes in v1:
time: 137 us
  Pallas kernels  132 us (96%)
  local copies, waits for them, and re-layouts  4.81 us (4%)
    pallas_call x1, Pallas kernels, fused_on_device(): pl.pallas_call(moe_kernel, out_shape=jax.ShapeDtypeStruct((rows, piece),...  132 us
    unnamed x3, local copies, waits for them, and re-layouts  4.81 us

profile of v1, /device:TPU:0, one launch (start us, length us, event | category | flops | bytes accessed | tf_op | source)
XLA Modules:
  0.0 136.9 jit_solution(4961187081479477099)
XLA Ops:
  0.0 1.5 %copy.9.ids_ref = s32[256,2]{1,0:T(8,128)} copy(s32[256,2]{0,1:T(2,128)} %param.9) | data formatting | bytes 4096 | tf_op args[1]
  1.5 1.5 %copy.10.gates_ref = f32[256,2]{1,0:T(8,128)} copy(f32[256,2]{0,1:T(2,128)} %param.10) | data formatting | bytes 4096 | tf_op args[2]
  2.9 132.1 %shard_map.82 = bf16[256,1024]{1,0:T(8,128)(2,1)} custom-call(s32[256,2]{1,0:T(8,128)} %copy.9.ids_ref, f32[256,2]{1,0:T(8,128)} %copy.10.gates_ref, f32[1,1024]{1,0:T(1,128)} %bitcast.2, f32[1,1024]{1,0:T(1,128)} %bitcast.3, bf16[256,4096]{1,0:T(8,128)(2,1)} %tokens_ref.1, bf16[4,4096,512]{2,1,0:T(8,128)(2,1)} %wg_ref.1, bf16[4,4096,512]{2,1,0:T(8,128)(2,1)} %wu_ref.1, ...), custom_call_target="tpu_custom_call" | custom-call | tf_op jit(solution)/shard_map/pallas_call | solution.py:375
  135.0 1.9 %copy.12 = bf16[256,1024]{1,0:T(8,128)(2,1)} copy(bf16[256,1024]{1,0:T(8,128)(2,1)} %shard_map.82) | data formatting | bytes 1048576

commit v2 on v1

--- a/solution.py
+++ b/solution.py
@@ -56,9 +56,12 @@
 
 
 GROUP_EXPERTS = 4
-CHUNKS = 8
+CHUNKS = 16
 HALF = CHUNKS // 2
-Z_OFFSETS = (2, 1, 3, 0)
+Z_OFFSETS = (2, 2, 1, 1, 3, 3, 0, 0)
+PIECES = 8
+SENT = 6
+LAG = 4
 F32 = jnp.float32
 BF16 = jnp.bfloat16
 MESH = pl.DeviceIdType.MESH
@@ -85,6 +88,7 @@
     experts = wg_ref.shape[0]
     cols = width // CHUNKS
     piece = gain_ref.shape[1]
+    part_cols = piece // 2
 
     def remote(src, dst, send, recv, e, t):
         return pltpu.make_async_remote_copy(
@@ -110,7 +114,7 @@
     def load_wd(i):
         q = (z + Z_OFFSETS[i]) % 4
         return pltpu.make_async_copy(
-            wd_ref.at[:, :, span(q, piece)], wd.at[i], wd_sem.at[i])
+            wd_ref.at[:, :, span(q * 2 + i % 2, part_cols)], wd.at[i], wd_sem.at[i])
 
     def direct(j):
         return par * HALF + j
@@ -169,7 +173,24 @@
     for d in (1, 2, 3):
         pl.semaphore_signal(
             barrier, inc=1, device_id={"ep": ep, "tp": (z + d) % 4}, device_id_type=MESH)
+    total_experts = 4 * experts
+    expert_row = lax.broadcasted_iota(jnp.int32, (total_experts, rows), 0)
+    first = ids_ref[0:1, :] == expert_row
+    second = ids_ref[1:2, :] == expert_row
+    named = jnp.where(first | second, 1.0, 0.0).astype(F32)
+    weight = jnp.where(first, gates_ref[0:1, :], jnp.where(second, gates_ref[1:2, :], 0.0))
+    tri_r = lax.broadcasted_iota(jnp.int32, (rows, rows), 0)
+    tri_c = lax.broadcasted_iota(jnp.int32, (rows, rows), 1)
+    before = jnp.where(tri_r < tri_c, 1.0, 0.0).astype(BF16)
+    position = jnp.dot(named.astype(BF16), before, preferred_element_type=F32)
+    slot = jnp.where(
+        named > 0.5, position + ((expert_row % experts) * CAP).astype(F32), -1.0)
+    for e in range(4):
+        meta[e, 0:experts, :] = slot[e * experts:(e + 1) * experts, :]
+        meta[e, experts:2 * experts, :] = weight[e * experts:(e + 1) * experts, :]
     pl.semaphore_wait(barrier, 6)
+    for k, e in enumerate(peers):
+        meta_copy(e, k).start()
 
     for j in range(HALF):
         load_tok(direct(j)).wait()
@@ -180,26 +201,9 @@
         own_copy(swapped(j)).start()
     for cp in load_w(direct(0), 0) + load_w(swapped(0), 1):
         cp.start()
-    for i in range(4):
+    for i in range(PIECES):
         load_wd(i).start()
 
-    lane = lax.broadcasted_iota(jnp.int32, (rows, 128), 1)
-    first = ids_ref[:, 0:1] == lane
-    second = ids_ref[:, 1:2] == lane
-    named = jnp.where(first | second, 1.0, 0.0).astype(F32)
-    weight = jnp.where(first, gates_ref[:, 0:1], jnp.where(second, gates_ref[:, 1:2], 0.0))
-    tri_r = lax.broadcasted_iota(jnp.int32, (rows, rows), 0)
-    tri_c = lax.broadcasted_iota(jnp.int32, (rows, rows), 1)
-    before = jnp.where(tri_c < tri_r, 1.0, 0.0).astype(BF16)
-    position = jnp.dot(before, named.astype(BF16), preferred_element_type=F32)
-    slot = jnp.where(named > 0.5, position + ((lane % experts) * CAP).astype(F32), -1.0)
-    slot_t = slot.T
-    weight_t = weight.T
-    for e in range(4):
-        meta[e, 0:experts, :] = slot_t[e * experts:(e + 1) * experts, :]
-        meta[e, experts:2 * experts, :] = weight_t[e * experts:(e + 1) * experts, :]
-    for k, e in enumerate(peers):
-        meta_copy(e, k).start()
     meta_in[ep] = meta[ep]
     acc[...] = jnp.zeros_like(acc)
     for k, e in enumerate(peers):
@@ -288,8 +292,8 @@
         q = (z + Z_OFFSETS[i]) % 4
         return remote(part.at[i, c, y], z_in.at[i], pz_send.at[i], pz_recv.at[i], ep, q)
 
-    for i in range(5):
-        if i < 4:
+    for i in range(PIECES + LAG):
+        if i < PIECES:
             load_wd(i).wait()
 
             def down(e, carry):
@@ -305,20 +309,25 @@
                 return carry
             lax.fori_loop(0, 4, gather, 0)
             core_copy(i).start()
-        if i >= 1:
+        if 1 <= i <= PIECES:
             core_copy(i - 1).wait_recv()
             part[i - 1, c, 1 - y] += core_in[i - 1, 1 - y]
             ret_copy(i - 1).start()
-
-    for i in range(3):
-        ret_copy(i).wait_recv()
-        part[i, c, y] += core_in[i, y] + y_in[i]
-        scatter_copy(i).start()
-    ret_copy(3).wait_recv()
-    total = (part[3, c, y] + core_in[3, y] + y_in[3]).astype(F32)
-    for i in range(3):
-        scatter_copy(i).wait_recv()
-        total += z_in[i].astype(F32)
+        if i >= LAG:
+            k = i - LAG
+            ret_copy(k).wait_recv()
+            part[k, c, y] += core_in[k, y] + y_in[k]
+            if k < SENT:
+                scatter_copy(k).start()
+
+    halves = []
+    for h in range(2):
+        half = part[SENT + h, c, y].astype(F32)
+        for i in range(h, SENT, 2):
+            scatter_copy(i).wait_recv()
+            half += z_in[i].astype(F32)
+        halves.append(half)
+    total = jnp.concatenate(halves, axis=1)
 
     local_mean = jnp.sum(total, axis=1, keepdims=True) * (1.0 / piece)
     gap = total - local_mean
@@ -355,10 +364,10 @@
         fwd_copy(ch).wait_send()
     for k, e in enumerate(peers):
         meta_copy(e, k).wait_send()
-    for i in range(4):
+    for i in range(PIECES):
         core_copy(i).wait_send()
         ret_copy(i).wait_send()
-    for i in range(3):
+    for i in range(SENT):
         scatter_copy(i).wait_send()
     for d in (1, 2, 3):
         stat_copy(d).wait_send()
@@ -369,6 +378,7 @@
     experts, _, hidden = w_gate.shape
     piece = norm_gain.shape[0]
     cols = width // CHUNKS
+    part_cols = piece // 2
     dma = pltpu.SemaphoreType.DMA
     vmem = pl.BlockSpec(memory_space=pltpu.VMEM)
     hbm = pl.BlockSpec(memory_space=pl.ANY)
@@ -380,32 +390,32 @@
         scratch_shapes=[
             pltpu.VMEM((CHUNKS, 4, rows, cols), BF16),
             pltpu.VMEM((2, 2, experts, cols, hidden), BF16),
-            pltpu.VMEM((4, experts, hidden, piece), BF16),
+            pltpu.VMEM((PIECES, experts, hidden, part_cols), BF16),
             pltpu.VMEM((2, experts, 4 * CAP, hidden), F32),
             pltpu.VMEM((experts, 4 * CAP, hidden), BF16),
             pltpu.VMEM((experts, 4 * CAP, cols), BF16),
-            pltpu.VMEM((4, experts * CAP, piece), BF16),
+            pltpu.VMEM((4, experts * CAP, part_cols), BF16),
             pltpu.VMEM((4, experts * CAP, rows), BF16),
             pltpu.VMEM((4, rows, experts * CAP), BF16),
             pltpu.VMEM((experts, 4 * CAP, 128), F32),
             pltpu.VMEM((4, 2 * experts, rows), F32),
             pltpu.VMEM((4, 2 * experts, rows), F32),
-            pltpu.VMEM((4, 2, 2, rows, piece), BF16),
-            pltpu.VMEM((4, 2, rows, piece), BF16),
-            pltpu.VMEM((4, rows, piece), BF16),
-            pltpu.VMEM((3, rows, piece), BF16),
+            pltpu.VMEM((PIECES, 2, 2, rows, part_cols), BF16),
+            pltpu.VMEM((PIECES, 2, rows, part_cols), BF16),
+            pltpu.VMEM((PIECES, rows, part_cols), BF16),
+            pltpu.VMEM((SENT, rows, part_cols), BF16),
             pltpu.VMEM((16, rows), F32),
             pltpu.VMEM((3, 16, rows), F32),
             dma((CHUNKS,)), dma((HALF,)), dma((HALF,)), dma((HALF,)), dma((HALF,)),
             dma((CHUNKS,)), dma((CHUNKS,)), dma((CHUNKS,)), dma((CHUNKS,)),
-            dma((3,)), dma((3,)), dma((2, 2)), dma((4,)),
-            dma((4,)), dma((4,)), dma((4,)), dma((4,)),
-            dma((3,)), dma((3,)), dma((3,)), dma((3,)),
+            dma((3,)), dma((3,)), dma((2, 2)), dma((PIECES,)),
+            dma((PIECES,)), dma((PIECES,)), dma((PIECES,)), dma((PIECES,)),
+            dma((SENT,)), dma((SENT,)), dma((3,)), dma((3,)),
         ],
         compiler_params=pltpu.CompilerParams(
             collective_id=0, has_side_effects=True, vmem_limit_bytes=64 * 1024 * 1024 - 65536),
     )(
-        expert_ids, gates, norm_gain[None, :], norm_bias[None, :],
+        expert_ids.T, gates.T, norm_gain[None, :], norm_bias[None, :],
         tokens, w_gate, w_up, w_down,
     )
 

time: 137 us -> 115 us (0.84)
  Pallas kernels: 132 us -> 113 us
  local copies, waits for them, and re-layouts: 4.81 us -> 1.87 us
    pallas_call x1, Pallas kernels: 132 us -> 113 us  [fused_on_device(): pl.pallas_call(moe_kernel, out_shape=jax.ShapeDtypeStruct((rows, piece),...]
    unnamed x3 -> x1, local copies, waits for them, and re-layouts: 4.81 us -> 1.87 us
where the time goes in v2:
time: 115 us
  Pallas kernels  113 us (98%)
  local copies, waits for them, and re-layouts  1.87 us (2%)
    pallas_call x1, Pallas kernels, fused_on_device(): pl.pallas_call(moe_kernel, out_shape=jax.ShapeDtypeStruct((rows, piece),...  113 us

profile of v2, /device:TPU:0, one launch (start us, length us, event | category | flops | bytes accessed | tf_op | source)
XLA Modules:
  0.0 114.7 jit_solution(10770879230539799901)
XLA Ops:
  0.0 112.8 %shard_map.82 = bf16[256,1024]{1,0:T(8,128)(2,1)} custom-call(s32[2,256]{1,0:T(2,128)} %bitcast.6, f32[2,256]{1,0:T(2,128)} %bitcast.7, f32[1,1024]{1,0:T(1,128)} %bitcast.4, f32[1,1024]{1,0:T(1,128)} %bitcast.5, bf16[256,4096]{1,0:T(8,128)(2,1)} %tokens_ref.1, bf16[4,4096,512]{2,1,0:T(8,128)(2,1)} %wg_ref.1, bf16[4,4096,512]{2,1,0:T(8,128)(2,1)} %wu_ref.1, ...), custom_call_target="tpu_custom_call" | custom-call | tf_op jit(solution)/shard_map/pallas_call | solution.py:385
  112.8 1.9 %copy.10 = bf16[256,1024]{1,0:T(8,128)(2,1)} copy(bf16[256,1024]{1,0:T(8,128)(2,1)} %shard_map.82) | data formatting | bytes 1048576
